TPU v7x, 32 devices: a whole 2x2x4 slice. The times are simulated.
32 devices in a mesh: sp: 8 (over z, y), tp: 4 (over x, core).
Axes of the slice: x: 2, y: 2, z: 4, core: 2. Of those that a mesh axis runs over, the one named last changes fastest.
Arguments:
- tokens: bfloat16 [4096, 2048], P('sp', 'tp'), may hold values from -64 to 64
- conv_input: bfloat16 [2048, 1024], P(None, 'tp'), may hold values from -0.125 to 0.125
- conv_inner: bfloat16 [2048, 1024], P(None, 'tp'), may hold values from -0.125 to 0.125
- conv_outer: bfloat16 [2048, 1024], P(None, 'tp'), may hold values from -0.125 to 0.125
- conv_gate: bfloat16 [2048, 1024], P(None, 'tp'), may hold values from -0.125 to 0.125
- conv_taps: bfloat16 [3, 1024], P(None, 'tp'), may hold values from -3.5 to 3.5
- query_proj: bfloat16 [2048, 1536], P(None, 'tp'), may hold values from -8 to 8
- latent_proj: bfloat16 [2048, 256], replicated, may hold values from -1 to 1
- rope_proj: bfloat16 [2048, 32], replicated, may hold values from -0.125 to 0.125
- latent_gain: float32 [256], replicated, may hold values from 0.1 to 1.9
- key_up: bfloat16 [256, 1024], P(None, 'tp'), may hold values from -2 to 2
- value_up: bfloat16 [256, 1024], P(None, 'tp'), may hold values from -0.375 to 0.375
- attn_gate: bfloat16 [2048, 1024], P(None, 'tp'), may hold values from -0.125 to 0.125
- conv_down: bfloat16 [1024, 2048], P('tp'), may hold values from -0.1875 to 0.1875
- attn_down: bfloat16 [1024, 2048], P('tp'), may hold values from -0.75 to 0.75
Outputs:
- layer_out: bfloat16 [4096, 2048], P(('sp', 'tp'))
All inputs are finite; a program needn't handle non-finite values.
Results may differ from a plain program's by a relative error of at most 0.014.
Values may be sent and summed in bfloat16 or wider, within the bound.
A program may use at most 128 MiB of HBM per device.

v0:
```python
import jax
import jax.numpy as jnp
from jax import lax
from jax.sharding import PartitionSpec as P

NOPE = 64
ROPE = 32
VDIM = 64
GRID_W = 64


rms_eps = 1e-06
rope_theta = 10000.0


def with_halo(cells, sides, width):
    for axis, dim in sides:
        count = lax.axis_size(axis)
        ends = count - 1
        head = lax.slice_in_dim(cells, 0, width, axis=dim)
        tail = lax.slice_in_dim(cells, cells.shape[dim] - width, cells.shape[dim], axis=dim)
        cells = jnp.concatenate(
            [
                lax.ppermute(tail, axis, [(i, (i + 1) % count) for i in range(ends)]),
                cells,
                lax.ppermute(head, axis, [((i + 1) % count, i) for i in range(ends)]),
            ],
            axis=dim,
        )
    return cells


def rounded(values):
    return lax.optimization_barrier(values.astype(jnp.bfloat16))


def axial_tables(positions, rope_width, grid_width):
    quarter = rope_width // 4
    frequency = rope_theta ** (-jnp.arange(quarter, dtype=jnp.float32) * 2.0 / (rope_width // 2))
    grid_row = (positions // grid_width).astype(jnp.float32)
    grid_col = (positions % grid_width).astype(jnp.float32)
    row_angle = grid_row[:, None] * frequency[None, :]
    col_angle = grid_col[:, None] * frequency[None, :]
    return (jnp.cos(row_angle), jnp.sin(row_angle), jnp.cos(col_angle), jnp.sin(col_angle))


def turn_half(vector, cos_table, sin_table):
    half_width = vector.shape[-1] // 2
    leading = vector[..., :half_width]
    trailing = vector[..., half_width:]
    return jnp.concatenate(
        [leading * cos_table - trailing * sin_table, trailing * cos_table + leading * sin_table],
        axis=-1,
    )


def axial_turn(vector, tables):
    half_width = vector.shape[-1] // 2
    return jnp.concatenate(
        [
            turn_half(vector[..., :half_width], tables[0], tables[1]),
            turn_half(vector[..., half_width:], tables[2], tables[3]),
        ],
        axis=-1,
    )


def on_device(
    tokens,
    conv_input,
    conv_inner,
    conv_outer,
    conv_gate,
    conv_taps,
    query_proj,
    latent_proj,
    rope_proj,
    latent_gain,
    key_up,
    value_up,
    attn_gate,
    conv_down,
    attn_down,
):
    tok_rows = tokens.shape[0]
    model_width = query_proj.shape[0]
    local_heads = key_up.shape[1] // NOPE
    in_weights = (
        conv_input,
        conv_inner,
        conv_outer,
        conv_gate,
        query_proj,
        latent_proj,
        rope_proj,
        attn_gate,
    )
    widened = tokens.astype(jnp.float32)
    squares = lax.psum(jnp.sum(widened * widened, axis=1), "tp")
    shard_piece = lax.all_gather(tokens, "tp", axis=1, tiled=True)
    new_terms = tuple(
        (jnp.dot(shard_piece, matrix, preferred_element_type=jnp.float32) for matrix in in_weights)
    )
    projected = tuple((right_sum for right_sum in new_terms))
    row_scale = lax.rsqrt(squares / model_width + rms_eps)[:, None]
    value_in, inner_in, outer_in, gate_in, queries, latent, rope_in, gate_attn = tuple(
        (proj_term * row_scale for proj_term in projected)
    )
    conv_product = (
        rounded(inner_in).astype(jnp.float32) * rounded(value_in).astype(jnp.float32)
    ).astype(jnp.bfloat16)
    padded = with_halo(conv_product, (("sp", 0),), 1).astype(jnp.float32)
    tap_weights = conv_taps.astype(jnp.float32)
    conv_mixed = (
        padded[:-2] * tap_weights[0] + padded[1:-1] * tap_weights[1] + padded[2:] * tap_weights[2]
    )
    conv_out = (
        jax.nn.silu(rounded(gate_in).astype(jnp.float32))
        * rounded(outer_in).astype(jnp.float32)
        * conv_mixed
    ).astype(jnp.bfloat16)
    positions = lax.axis_index("sp") * tok_rows + jnp.arange(tok_rows, dtype=jnp.int32)
    tables = axial_tables(positions, ROPE, GRID_W)
    queries = queries.reshape(tok_rows, local_heads, NOPE + ROPE)
    query_nope = queries[..., :NOPE].astype(jnp.bfloat16)
    query_rope = axial_turn(
        queries[..., NOPE:], tuple((grid_table[:, None, :] for grid_table in tables))
    ).astype(jnp.bfloat16)
    latent = (
        latent * lax.rsqrt(jnp.mean(latent * latent, axis=1, keepdims=True) + rms_eps) * latent_gain
    ).astype(jnp.bfloat16)
    key_rope = axial_turn(rope_in, tables).astype(jnp.bfloat16)
    score_scale = (NOPE + ROPE) ** (-0.5)
    initial = (
        jnp.full((tok_rows, local_heads), -jnp.inf, jnp.float32),
        jnp.zeros((tok_rows, local_heads), jnp.float32),
        jnp.zeros((tok_rows, local_heads, VDIM), jnp.float32),
    )
    latent_piece = lax.all_gather(latent, "sp", axis=0, tiled=True)
    rope_piece = lax.all_gather(key_rope, "sp", axis=0, tiled=True)
    key_count = latent_piece.shape[0]
    span_rows = key_count
    while span_rows > 1024 and span_rows % 2 == 0:
        span_rows = span_rows // 2

    def one_span(state_now, span_start):
        latent_span = lax.dynamic_slice_in_dim(latent_piece, span_start, span_rows, 0)
        rope_span = lax.dynamic_slice_in_dim(rope_piece, span_start, span_rows, 0)
        key_nope = (
            jnp.dot(latent_span, key_up, preferred_element_type=jnp.float32)
            .astype(jnp.bfloat16)
            .reshape(span_rows, local_heads, NOPE)
        )
        key_values = (
            jnp.dot(latent_span, value_up, preferred_element_type=jnp.float32)
            .astype(jnp.bfloat16)
            .reshape(span_rows, local_heads, VDIM)
        )
        scores = jnp.einsum(
            "qhd,khd->qhk", query_nope, key_nope, preferred_element_type=jnp.float32
        )
        scores = (
            scores
            + jnp.einsum("qhd,kd->qhk", query_rope, rope_span, preferred_element_type=jnp.float32)
        ) * score_scale
        row_top, weight_total, weighted = state_now
        new_top = jnp.maximum(row_top, jnp.max(scores, axis=2))
        weights = jnp.exp(scores - new_top[:, :, None])
        shrink = jnp.exp(row_top - new_top)
        weight_total = weight_total * shrink + jnp.sum(weights, axis=2)
        weighted = weighted * shrink[:, :, None] + jnp.einsum(
            "qhk,khd->qhd",
            weights.astype(jnp.bfloat16),
            key_values,
            preferred_element_type=jnp.float32,
        )
        return ((new_top, weight_total, weighted), None)

    span_starts = jnp.arange(key_count // span_rows, dtype=jnp.int32) * span_rows
    gathered_state = lax.scan(one_span, initial, span_starts)[0]
    attended = (gathered_state[2] / gathered_state[1][:, :, None]).reshape(
        tok_rows, local_heads * VDIM
    )
    attn_out = (jax.nn.silu(rounded(gate_attn).astype(jnp.float32)) * attended).astype(jnp.bfloat16)
    return lax.psum_scatter(
        (
            jnp.dot(conv_out, conv_down, preferred_element_type=jnp.float32)
            + jnp.dot(attn_out, attn_down, preferred_element_type=jnp.float32)
        ).astype(jnp.bfloat16),
        "tp",
        scatter_dimension=0,
        tiled=True,
    )


def solution(mesh):
    placed = (
        P("sp", "tp"),
        P(None, "tp"),
        P(None, "tp"),
        P(None, "tp"),
        P(None, "tp"),
        P(None, "tp"),
        P(None, "tp"),
        P(),
        P(),
        P(),
        P(None, "tp"),
        P(None, "tp"),
        P(None, "tp"),
        P("tp", None),
        P("tp", None),
    )
    return jax.shard_map(
        on_device, mesh=mesh, in_specs=placed, out_specs=P(("sp", "tp"), None), check_vma=False
    )
```

profile of v0, /device:TPU:0, one launch (start us, length us, event | category | flops | bytes accessed | tf_op | source)
XLA Modules:
  0.0 174.0 jit_solution(3789378869783381804)
XLA Ops:
  8.6 8.4 %psum.7 = f32[512]{0:T(512)S(1)} all-reduce(f32[512]{0:T(512)S(1)} %multiply_reduce_fusion), channel_id=1, replica_groups=mesh['sp'=8,'tp'=4] {'tp'}, use_global_device_ids=true, to_apply=%region_1.0 | all-reduce | flops 512 | bytes 4096 | tf_op jit(solution)/shard_map/psum | solution.py:99
  17.8 16.4 %all-gather.3.cloned.1.call-done = bf16[512,2048]{1,0:T(8,128)(2,1)} async-done(((bf16[512,512]{1,0:T(8,128)(2,1)}), bf16[512,2048]{1,0:T(8,128)(2,1)}) %all-gather.3.cloned.1.call-update) | async-done | bytes 2097168 | tf_op jit(solution)/shard_map/all_gather | solution.py:100
  34.2 2.6 %multiply_reduce_fusion.1 = (f32[512]{0:T(512)S(1)}, f32[512,256]{1,0:T(8,128)S(1)}) fusion(f32[512]{0:T(512)S(1)} %add_rsqrt_fusion.1, bf16[512,2048]{1,0:T(8,128)(2,1)} %all-gather.3.cloned.1.call-done, bf16[2048,256]{1,0:T(8,128)(2,1)} %param.24), kind=kOutput, calls=%fused_computation.58 | convolution fusion | flops 537263616 | bytes 3674112 | tf_op jit(solution)/shard_map/dot_general | solution.py:102
  37.8 2.7 %fusion.22 = bf16[512,256]{1,0:T(8,128)(2,1)S(1)} fusion(bf16[512,2048]{1,0:T(8,128)(2,1)} %all-gather.3.cloned.1.call-done, bf16[2048,256]{1,0:T(8,128)(2,1)} %param.19, f32[512]{0:T(512)S(1)} %add_rsqrt_fusion.1), kind=kOutput, calls=%fused_computation.33 | convolution fusion | flops 537133056 | bytes 3409920 | tf_op jit(solution)/shard_map/dot_general | solution.py:102
  41.4 3.4 %collective-permute-start = (bf16[1,256]{1,0:T(2,128)(2,1)S(1)}, bf16[1,256]{1,0:T(2,128)(2,1)S(1)}, u32[]{:S(2)}, u32[]{:S(2)}) collective-permute-start(bf16[1,256]{1,0:T(2,128)(2,1)S(1)} %get-tuple-element.133), channel_id=1, source_target_pairs={{0,4},{4,8},{8,12},{12,16},{16,20},{20,24},{24,28},{1,5},{5,9},{9,... | collective-permute-start | bytes 1544 | tf_op jit(solution)/shard_map/ppermute | solution.py:24
  51.5 34.1 %all_gather.11 = bf16[4096,32]{0,1:T(8,128)(2,1)S(1)} all-gather(bf16[512,32]{0,1:T(8,128)(2,1)S(1)} %pad_maximum_fusion.1), channel_id=1, replica_groups=mesh['sp'=8,'tp'=4] {'sp'}, dimensions={0}, use_global_device_ids=true | all-gather | bytes 294912 | tf_op jit(solution)/shard_map/all_gather | solution.py:140
  85.8 2.9 %fusion.38 = f32[512,2048]{1,0:T(8,128)} fusion(bf16[256,2048]{1,0:T(8,128)(2,1)S(1)} %copy-done.4, f32[514,256]{1,0:T(8,128)S(1)} %maximum_convert_fusion, bf16[512,256]{1,0:T(8,128)(2,1)S(1)} %fusion.21, bf16[512,256]{1,0:T(8,128)(2,1)S(1)} %fusion.20, f32[256]{0:T(256)S(1)} %bitcast.76, f32[256]{0:T(256)S(1)} %bitcast.75, f32[256]{0:T(256)S(1)} %bitcast.74), kind=kOutput, calls=%fused_computation.63 | convolution fusion | flops 538705920 | bytes 7343104 | tf_op jit(solution)/shard_map/dot_general | solution.py:187
  89.5 43.0 %while.15 = (s32[]{:T(128)}, f32[512,4]{0,1:T(4,128)S(1)}, f32[512,4]{0,1:T(4,128)S(1)}, f32[512,4,64]{0,2,1:T(8,128)S(1)}, s32[4]{0:T(128)S(1)}, /*index=5*/bf1...) while((s32[]{:T(128)}, f32[512,4]{0,1:T(4,128)S(1)}, ...), condition=%wide.region_6.7_spmd.clone, body=%wide.region_3.6_spmd.clone.sunk | while | flops 955131904 | bytes 46989520 | solution.py:180
  93.4 1.4 convolution_convert_fusion.4
  96.1 1.4 fusion.105
  98.7 1.5 fusion.108
  102.8 1.4 convolution_convert_fusion.5
  104.2 1.4 convolution_convert_fusion.4
  106.9 1.4 fusion.105
  109.5 1.5 fusion.108
  113.5 1.4 convolution_convert_fusion.5
  114.9 1.4 convolution_convert_fusion.4
  117.6 1.4 fusion.105
  120.2 1.5 fusion.108
  125.7 1.4 convolution_convert_fusion.4
  128.4 1.4 fusion.105
  131.0 1.5 fusion.108
  132.8 4.6 %add_convert_fusion = bf16[512,2048]{1,0:T(8,128)(2,1)} fusion(f32[512,2048]{1,0:T(8,128)} %fusion.38, bf16[256,2048]{1,0:T(8,128)(2,1)} %param.31, f32[512,256]{1,0:T(8,128)S(1)} %copy.21, bf16[512,256]{1,0:T(8,128)(2,1)S(1)} %fusion.24), kind=kOutput, calls=%fused_computation.23 | convolution fusion | flops 539885568 | bytes 8126464 | tf_op jit(solution)/shard_map/dot_general | solution.py:188
  137.4 30.1 %reduce-scatter.2.cloned.1.call-done = bf16[128,2048]{1,0:T(8,128)(2,1)} async-done(((bf16[512,2048]{1,0:T(8,128)(2,1)}), bf16[128,2048]{1,0:T(8,128)(2,1)}) %reduce-scatter.2.cloned.1.call-update) | async-done | bytes 524304 | tf_op jit(solution)/shard_map/reduce_scatter | solution.py:185
  (85 shorter events, 27.2 us)
Async XLA Ops:
  6.5 40.5 %copy-start = (bf16[2048,384]{1,0:T(8,128)(2,1)S(1)}, bf16[2048,384]{1,0:T(8,128)(2,1)}, u32[]{:S(2)}) copy-start(bf16[2048,384]{1,0:T(8,128)(2,1)} %param.23) | copy-start | bytes 4718596
  6.5 27.7 %all-gather.3.cloned.1.call-start = ((), (), s32[]{:S(2)}) async-start(), calls=%async_computation.1 | async-start | bytes 2621440 | tf_op jit(solution)/shard_map/all_gather | solution.py:100
  7.3 82.2 %all-gather.5.cloned.1.call-start = ((), (), s32[]{:S(2)}) async-start(), calls=%async_computation.2 | async-start | bytes 2359296 | tf_op jit(solution)/shard_map/all_gather | solution.py:139
  17.8 19.1 %copy-start.6 = (f32[256]{0:T(256)S(1)}, f32[256]{0:T(256)}, u32[]{:S(2)}) copy-start(f32[256]{0:T(256)} %param.26) | copy-start | bytes 3076
  37.7 129.7 %reduce-scatter.2.cloned.1.call-start = ((), (), s32[]{:S(2)}) async-start(), calls=%async_computation.3 | async-start | bytes 2621440 | tf_op jit(solution)/shard_map/reduce_scatter | solution.py:185
  37.8 2.7 %copy-start.3 = (bf16[512,2048]{1,0:T(8,128)(2,1)S(1)}, bf16[512,2048]{1,0:T(8,128)(2,1)}, u32[]{:S(2)}) copy-start(bf16[512,2048]{1,0:T(8,128)(2,1)} %all-gather.3.cloned.1.call-done) | copy-start | bytes 6291460
  37.8 2.8 %copy-start.7 = (bf16[2048,256]{1,0:T(8,128)(2,1)S(1)}, bf16[2048,256]{1,0:T(8,128)(2,1)}, u32[]{:S(2)}) copy-start(bf16[2048,256]{1,0:T(8,128)(2,1)} %param.18) | copy-start | bytes 3145732
  40.6 5.5 %copy-start.5 = (bf16[2048,32]{0,1:T(8,128)(2,1)S(1)}, bf16[2048,32]{0,1:T(8,128)(2,1)}, u32[]{:S(2)}) copy-start(bf16[2048,32]{0,1:T(8,128)(2,1)} %param.25) | copy-start | bytes 393220
  41.4 44.3 %collective-permute-start = (bf16[1,256]{1,0:T(2,128)(2,1)S(1)}, bf16[1,256]{1,0:T(2,128)(2,1)S(1)}, u32[]{:S(2)}, u32[]{:S(2)}) collective-permute-start(bf16[1,256]{1,0:T(2,128)(2,1)S(1)} %get-tuple-element.133), channel_id=1, source_target_pairs={{0,4},{4,8},{8,12},{12,16},{16,20},{20,24},{24,28},{1,5},{5,9},{9,... | collective-permute-start | bytes 1544 | tf_op jit(solution)/shard_map/ppermute | solution.py:24
  44.8 40.9 %collective-permute-start.1 = (bf16[1,256]{1,0:T(2,128)(2,1)S(1)}, bf16[1,256]{1,0:T(2,128)(2,1)S(1)}, u32[]{:S(2)}, u32[]{:S(2)}) collective-permute-start(bf16[1,256]{1,0:T(2,128)(2,1)S(1)} %get-tuple-element.134), channel_id=1, source_target_pairs={{4,0},{8,4},{12,8},{16,12},{20,16},{24,20},{28,24},{5,1},{9,5},{13... | collective-permute-start | bytes 1544 | tf_op jit(solution)/shard_map/ppermute | solution.py:26
  47.1 1.2 copy-start.8
  48.3 1.2 copy-start.9
  49.5 1.2 copy-start.10
  51.5 34.3 %copy-start.4 = (bf16[256,2048]{1,0:T(8,128)(2,1)S(1)}, bf16[256,2048]{1,0:T(8,128)(2,1)}, u32[]{:S(2)}) copy-start(bf16[256,2048]{1,0:T(8,128)(2,1)} %param.30) | copy-start | bytes 3145732
  85.8 3.7 %copy-start.1 = (bf16[256,256]{1,0:T(8,128)(2,1)S(1)}, bf16[256,256]{1,0:T(8,128)(2,1)}, u32[]{:S(2)}) copy-start(bf16[256,256]{1,0:T(8,128)(2,1)} %param.27) | copy-start | bytes 393220
  85.8 3.7 %copy-start.2 = (bf16[256,256]{1,0:T(8,128)(2,1)S(1)}, bf16[256,256]{1,0:T(8,128)(2,1)}, u32[]{:S(2)}) copy-start(bf16[256,256]{1,0:T(8,128)(2,1)} %param.28) | copy-start | bytes 393220
Sparse Core Ops, SparseCore 0:
  8.9 25.2 all-gather.2
  37.9 51.5 all-gather.4
  137.5 29.9 reduce-scatter.1
where the time goes:
time: 175 us; the launch traced here: 174 us
  waiting for transfers between devices  48.1 us (27%)
  matrix products  45.5 us (26%)
  blocking collectives  42.5 us (24%)
  between operations  13.4 us (8%)
  loops' own time  8.05 us (5%)
  other arithmetic  7.14 us (4%)
  starting transfers between devices  4.75 us (3%)
  local copies, waits for them, and re-layouts  4.6 us (3%)
    all_gather x1, blocking collectives, on_device(): rope_piece = lax.all_gather(key_rope, 'sp', axis=0, tiled=True)  34.1 us
    reduce_scatter x1, waiting for transfers between devices, on_device(): lax.psum_scatter((jnp.dot(conv_out, conv_down, preferred_element_type=jnp...  30.1 us
    all_gather x1, waiting for transfers between devices, on_device(): shard_piece = lax.all_gather(tokens, 'tp', axis=1, tiled=True)  16.4 us
    dot_general x8, matrix products, on_device(): jnp.dot(shard_piece, matrix, preferred_element_type=jnp.float32)  9.98 us
    psum x1, blocking collectives, on_device(): squares = lax.psum(jnp.sum(widened * widened, axis=1), 'tp')  8.37 us
    another operation x1, loops' own time, on_device(): gathered_state = lax.scan(one_span, initial, span_starts)[0]  8.05 us
    dot_general x4, matrix products, one_span(): jnp.einsum('qhk,khd->qhd', weights.astype(jnp.bfloat16), key_values, pref...  5.94 us
    dot_general x4, matrix products, one_span(): jnp.einsum('qhd,kd->qhk', query_rope, rope_span, preferred_element_type=j...  5.76 us
  transfers between devices with their start and end apart: 5, of which 3 were waited for; matrix products, arithmetic and copies ran while one was open for 7% of the time, Pallas kernels for 0%

commit v1 on v0

v1 whole, which is shorter than its diff:
```python
import functools
import math

import jax
import jax.numpy as jnp
from jax import lax
from jax.experimental import pallas as pl
from jax.experimental.pallas import tpu as pltpu
from jax.sharding import PartitionSpec as P

NOPE = 64
ROPE = 32
VDIM = 64
GRID_W = 64
LANES = 128
rms_eps = 1e-06
rope_theta = 10000.0
MESH = pl.DeviceIdType.MESH
BF = jnp.bfloat16
F32 = jnp.float32


def silu(v):
    return v / (1.0 + jnp.exp(-v))


def dot(a, b):
    return jnp.dot(a, b, preferred_element_type=F32)


def body(
    dims,
    tokens, wci, wcn, wco, wcg, wq, wg, wl, wr, cd, ad, taps, gain, ku, vu,
    out,
    x_all, w_conv, w_q, w_g, w_lr, w_down, kv, kbuf, vbuf, qbuf, scl, cosb, sina, sinb,
    cprod, cgo, gat, halo, mix, mbuf, acc, sbuf, pbuf, xbuf, rbuf, ybuf,
    wsem, tsend, trecv, rsend, rrecv, ksend, krecv, psend, precv, hsend, hrecv,
    dsend, drecv, xsend, xrecv,
):
    n_sp, n_tp, R, fl, D, H, C, KV, NC = dims
    X = n_tp // 2
    RG = R // X
    TB = R // n_tp
    RC = R // NC
    HB = R // 2
    HR = HB // 8
    sp = lax.axis_index("sp")
    tp = lax.axis_index("tp")
    chip = tp // 2
    core = tp % 2
    mate = chip * 2 + (1 - core)

    loads = [
        pltpu.make_async_copy(wl, w_lr.at[:, 0:KV], wsem.at[0]),
        pltpu.make_async_copy(wr, w_lr.at[:, KV:KV + LANES], wsem.at[1]),
        pltpu.make_async_copy(wcn, w_conv.at[0], wsem.at[2]),
        pltpu.make_async_copy(wci, w_conv.at[1], wsem.at[3]),
        pltpu.make_async_copy(wco, w_conv.at[2], wsem.at[4]),
        pltpu.make_async_copy(wcg, w_conv.at[3], wsem.at[5]),
        pltpu.make_async_copy(wq, w_q, wsem.at[6]),
        pltpu.make_async_copy(wg, w_g, wsem.at[7]),
        pltpu.make_async_copy(cd, w_down.at[0:C, :], wsem.at[8]),
        pltpu.make_async_copy(ad, w_down.at[C:, :], wsem.at[9]),
    ]

    def cols(j):
        return pl.ds(pl.multiple_of(j * fl, fl), fl)

    own = pltpu.make_async_copy(tokens, x_all.at[:, cols(tp)], wsem.at[10])

    barrier = pltpu.get_barrier_semaphore()
    pl.semaphore_signal(barrier, inc=1, device_id={"tp": mate}, device_id_type=MESH)
    for d in range(1, X):
        peer = ((chip + d) % X) * 2 + core
        pl.semaphore_signal(barrier, inc=1, device_id={"tp": peer}, device_id_type=MESH)
    for d in range(1, n_sp):
        pl.semaphore_signal(barrier, inc=1, device_id={"sp": (sp + d) % n_sp}, device_id_type=MESH)
    own.start()
    pl.semaphore_wait(barrier, 1 + (X - 1) + (n_sp - 1))

    def send_tok(d, c):
        peer = mate if d == 0 else ((chip + d) % X) * 2 + core
        rows = pl.ds(c * RC, RC)
        return pltpu.make_async_remote_copy(
            src_ref=tokens.at[rows], dst_ref=x_all.at[rows, cols(tp)],
            send_sem=tsend.at[d, c], recv_sem=trecv.at[d, c],
            device_id={"tp": peer}, device_id_type=MESH)

    def relay_tok(d, c):
        origin = ((chip - d + X) % X) * 2 + core
        rows = pl.ds(c * RC, RC)
        part = x_all.at[rows, cols(origin)]
        return pltpu.make_async_remote_copy(
            src_ref=part, dst_ref=part,
            send_sem=rsend.at[d, c], recv_sem=rrecv.at[d, c],
            device_id={"tp": mate}, device_id_type=MESH)

    for c in range(NC):
        for d in range(1, X):
            send_tok(d, c).start()
    for c in range(NC):
        send_tok(0, c).start()
    for w in loads:
        w.start()

    lane = lax.broadcasted_iota(jnp.int32, (R, LANES), 1)
    pos = sp * R + lax.broadcasted_iota(jnp.int32, (R, LANES), 0)
    rl = lane - NOPE
    grid = jnp.where(rl < ROPE // 2, pos // GRID_W, pos % GRID_W).astype(F32)
    freq = jnp.exp((lane % 8).astype(F32) * (-math.log(rope_theta) / 8.0))
    ang = grid * freq
    active = (lane >= NOPE) & (lane < NOPE + ROPE)
    first = (lane % 16) < 8
    sin = jnp.sin(ang)
    cosb[...] = jnp.where(active, jnp.cos(ang), 0.0)
    sina[...] = jnp.where(active & first, -sin, 0.0)
    sinb[...] = jnp.where(active & (~first), sin, 0.0)

    def turned(v, rows):
        return (pltpu.roll(v, LANES - 8, 1) * sina[rows, :]
                + pltpu.roll(v, 8, 1) * sinb[rows, :])

    own.wait()
    loads[0].wait()
    loads[1].wait()
    for c in range(NC):
        for d in range(1, X):
            send_tok(d, c).wait_recv()
            relay_tok(d, c).start()
        send_tok(0, c).wait_recv()
        for d in range(1, X):
            relay_tok(d, c).wait_recv()
        rows = pl.ds(c * RC, RC)
        xr = x_all[rows, :]
        xf = xr.astype(F32)
        sc = lax.rsqrt(jnp.sum(xf * xf, axis=1, keepdims=True) * (1.0 / D) + rms_eps)
        scl[rows, :] = jnp.broadcast_to(sc, (RC, LANES))
        z = dot(xr, w_lr[...]) * sc
        lat = z[:, :KV]
        lat = lat * lax.rsqrt(jnp.mean(lat * lat, axis=1, keepdims=True) + rms_eps) * gain[...]
        half, off = (c * RC) // HB, (c * RC) % HB
        kv[sp, half, off:off + RC, :] = lat.astype(BF)
        rp = z[:, KV:]
        mix[rows, 0:LANES] = rp * cosb[rows, :] + turned(rp, rows)
    for half in range(2):
        packed = []
        for g in range(2):
            total = jnp.zeros((HR, LANES), F32)
            for b in range(4):
                r0 = half * HB + (g * 4 + b) * HR
                total = total + pltpu.roll(mix[r0:r0 + HR, 0:LANES], (32 * b - NOPE) % LANES, 1)
            packed.append(total)
        kv[sp, half, HB:HB + HR, :] = jnp.concatenate(packed, axis=1).astype(BF)

    def send_kv(d):
        part = kv.at[sp, core]
        return pltpu.make_async_remote_copy(
            src_ref=part, dst_ref=part, send_sem=ksend.at[d], recv_sem=krecv.at[sp],
            device_id={"sp": (sp + d) % n_sp}, device_id_type=MESH)

    def recv_kv(o):
        part = kv.at[o, core]
        return pltpu.make_async_remote_copy(
            src_ref=part, dst_ref=part, send_sem=ksend.at[0], recv_sem=krecv.at[o],
            device_id={"tp": mate}, device_id_type=MESH)

    def relay_kv(o, which):
        part = kv.at[o, which]
        return pltpu.make_async_remote_copy(
            src_ref=part, dst_ref=part, send_sem=psend.at[o], recv_sem=precv.at[o],
            device_id={"tp": mate}, device_id_type=MESH)

    order = []
    for i in range(1, n_sp):
        order.append((i + 1) // 2 if i % 2 else n_sp - i // 2)
    for d in order:
        send_kv(d).start()

    for w in loads[2:6]:
        w.wait()
    PB = min(R, 256)

    @pl.loop(0, R // PB)
    def _(i):
        rows = pl.ds(pl.multiple_of(i * PB, PB), PB)
        xr = x_all[rows, :]
        sc = scl[rows, 0:1]
        inner = (dot(xr, w_conv[0]) * sc).astype(BF).astype(F32)
        value = (dot(xr, w_conv[1]) * sc).astype(BF).astype(F32)
        cprod[rows, :] = (inner * value).astype(BF)
        outer = (dot(xr, w_conv[2]) * sc).astype(BF).astype(F32)
        gate = (dot(xr, w_conv[3]) * sc).astype(BF).astype(F32)
        cgo[rows, :] = silu(gate) * outer

    EDGE = 16

    def send_halo(k):
        src = cprod.at[pl.ds(R - EDGE, EDGE)] if k == 0 else cprod.at[pl.ds(0, EDGE)]
        to = (sp + 1) % n_sp if k == 0 else (sp + n_sp - 1) % n_sp
        return pltpu.make_async_remote_copy(
            src_ref=src, dst_ref=halo.at[k], send_sem=hsend.at[k], recv_sem=hrecv.at[k],
            device_id={"sp": to}, device_id_type=MESH)

    send_halo(0).start()
    send_halo(1).start()
    loads[6].wait()
    loads[7].wait()

    @pl.loop(0, R // PB)
    def _(i):
        rows = pl.ds(pl.multiple_of(i * PB, PB), PB)
        xr = x_all[rows, :]
        sc = scl[rows, 0:1]
        q = dot(xr, w_q[...]) * sc
        ln = lax.broadcasted_iota(jnp.int32, (PB, LANES), 1)
        for h in range(H):
            v = q[:, h * LANES:(h + 1) * LANES]
            v = v * jnp.where(ln < NOPE, 1.0, cosb[rows, :]) + turned(v, rows)
            qbuf[h, rows, :] = v.astype(BF)
        gat[rows, :] = silu((dot(xr, w_g[...]) * sc).astype(BF).astype(F32))

    def build(o):
        ln = lax.broadcasted_iota(jnp.int32, (HR, LANES), 1)
        keep = (ln >= NOPE) & (ln < NOPE + ROPE)
        ones = jnp.where(lax.broadcasted_iota(jnp.int32, (HB, LANES), 1) == VDIM, 1.0, 0.0)
        for half in range(2):
            lat = kv[o, half, 0:HB, :]
            packed = kv[o, half, HB:HB + HR, :].astype(F32)
            parts = []
            for g in range(2):
                pg = packed[:, g * LANES:(g + 1) * LANES]
                for b in range(4):
                    parts.append(jnp.where(keep, pltpu.roll(pg, (NOPE - 32 * b) % LANES, 1), 0.0))
            rope = jnp.concatenate(parts, axis=0)
            k = dot(lat, ku[...])
            v = dot(lat, vu[...])
            rows = pl.ds(pl.multiple_of(o * R + half * HB, HB), HB)
            for h in range(H):
                kbuf[h, rows, :] = (k[:, h * LANES:(h + 1) * LANES] + rope).astype(BF)
                vbuf[h, rows, :] = (v[:, h * LANES:(h + 1) * LANES] + ones).astype(BF)

    scale = (NOPE + ROPE) ** -0.5

    def attend(row0, key0, count):
        qrows = pl.ds(row0, RG)
        krows = pl.ds(key0, count)
        for h in range(H):
            s = lax.dot_general(qbuf[h, qrows, :], kbuf[h, krows, :], (((1,), (1,)), ((), ())),
                                preferred_element_type=F32)
            old = mbuf[h]
            new = jnp.maximum(old, jnp.max(s, axis=1, keepdims=True))
            p = jnp.exp((s - new[:, 0:1]) * scale)
            shrink = jnp.exp((old - new) * scale)
            acc[h] = acc[h] * shrink + dot(p.astype(BF), vbuf[h, krows, :])
            mbuf[h] = new

    def reset():
        mbuf[...] = jnp.full(mbuf.shape, -jnp.inf, F32)
        acc[...] = jnp.zeros(acc.shape, F32)

    def finish(row0):
        rows = pl.ds(row0, RG)
        heads = []
        for h in range(H):
            a = acc[h]
            heads.append(a[:, :VDIM] / a[:, VDIM:VDIM + 1])
        attended = jnp.concatenate(heads, axis=1)
        mix[rows, C:] = gat[rows, :] * attended

    def row_of(k):
        return pl.multiple_of(k * RG, RG)

    def origin(s):
        step = jnp.where(s % 2 == 1, (s + 1) // 2, n_sp - s // 2)
        return (sp + step) % n_sp

    def block(k, which):
        rows = pl.ds(pl.multiple_of(k * RG + which * TB, TB), TB)
        return dot(mix[rows, :].astype(BF), w_down[...])

    def send_mate(d):
        return pltpu.make_async_remote_copy(
            src_ref=sbuf.at[d], dst_ref=pbuf.at[d], send_sem=dsend.at[d], recv_sem=drecv.at[d],
            device_id={"tp": mate}, device_id_type=MESH)

    def send_x(d):
        return pltpu.make_async_remote_copy(
            src_ref=xbuf.at[d], dst_ref=rbuf.at[d], send_sem=xsend.at[d], recv_sem=xrecv.at[d],
            device_id={"tp": ((chip + d) % X) * 2 + core}, device_id_type=MESH)

    def project_out(d):
        k = (chip + d) % X
        sbuf[d] = block(k, 1 - core).astype(BF)
        send_mate(d).start()
        ybuf[...] = block(k, core).astype(BF)

    def pair_sum(d):
        send_mate(d).wait_recv()
        return ybuf[...].astype(F32) + pbuf[d].astype(F32)

    first_chip = row_of((chip + 1) % X)
    reset()
    build(sp)
    attend(first_chip, pl.multiple_of(sp * R, R), R)

    o1 = origin(1)
    recv_kv(o1).wait_recv()
    relay_kv(o1, core).start()

    @pl.loop(1, n_sp)
    def _(s):
        o = origin(s)

        @pl.when(s + 1 < n_sp)
        def _():
            nxt = origin(s + 1)
            recv_kv(nxt).wait_recv()
            relay_kv(nxt, core).start()

        relay_kv(o, 1 - core).wait_recv()
        build(o)
        attend(first_chip, pl.multiple_of(o * R, R), R)

    finish(first_chip)

    send_halo(0).wait_recv()
    send_halo(1).wait_recv()
    cp = cprod[...].astype(F32)
    rid = lax.broadcasted_iota(jnp.int32, (R, C), 0)
    before = halo[0].astype(F32)[EDGE - 1:EDGE, :] * jnp.where(sp == 0, 0.0, 1.0)
    after = halo[1].astype(F32)[0:1, :] * jnp.where(sp == n_sp - 1, 0.0, 1.0)
    up = jnp.where(rid == 0, before, pltpu.roll(cp, 1, 0))
    down = jnp.where(rid == R - 1, after, pltpu.roll(cp, R - 1, 0))
    tw = taps[...].astype(F32)
    mix[:, 0:C] = cgo[...] * (up * tw[0:1] + cp * tw[1:2] + down * tw[2:3])

    loads[8].wait()
    loads[9].wait()
    CH = 2 if n_sp % 2 == 0 else 1
    for d in range(1, X + 1):
        e = d % X
        if X > 1:
            if d > 1:
                row0 = row_of((chip + e) % X)
                reset()

                @pl.loop(0, n_sp // CH)
                def _(s):
                    @pl.when(s == 1)
                    def _():
                        xbuf[d - 1] = pair_sum(d - 1).astype(BF)
                        send_x(d - 1).start()

                    attend(row0, pl.multiple_of(s * (CH * R), CH * R), CH * R)

                finish(row0)
        project_out(e)

    total = pair_sum(0)
    for d in range(1, X):
        send_x(d).wait_recv()
        total = total + rbuf[d].astype(F32)
    out[...] = total.astype(BF)

    for c in range(NC):
        send_tok(0, c).wait_send()
        for d in range(1, X):
            send_tok(d, c).wait_send()
            relay_tok(d, c).wait_send()
    for d in range(1, n_sp):
        send_kv(d).wait_send()
        relay_kv((sp + d) % n_sp, core).wait_send()
    send_halo(0).wait_send()
    send_halo(1).wait_send()
    for d in range(X):
        send_mate(d).wait_send()
    for d in range(1, X):
        send_x(d).wait_send()


def on_device(n_sp, n_tp, tokens, wci, wcn, wco, wcg, taps, wq, wl, wr, gain, ku, vu, wg, cd, ad):
    R, fl = tokens.shape
    D, C = wci.shape
    KV = wl.shape[1]
    H = ku.shape[1] // NOPE
    A = H * VDIM
    X = n_tp // 2
    RG, TB = R // X, R // n_tp
    NC = 4

    def by_head(w, width):
        w = w.reshape(w.shape[0], H, width)
        return jnp.pad(w, ((0, 0), (0, 0), (0, LANES - width))).reshape(w.shape[0], H * LANES)

    wq = by_head(wq, NOPE + ROPE)
    ku = by_head(ku, NOPE)
    vu = by_head(vu, VDIM)
    wr = jnp.pad(wr, ((0, 0), (NOPE, LANES - NOPE - ROPE)))
    HB = R // 2
    RB = HB + HB // 8
    S = n_sp * R
    dma = pltpu.SemaphoreType.DMA
    anys = pl.BlockSpec(memory_space=pl.ANY)
    vm = pl.BlockSpec(memory_space=pltpu.VMEM)
    V = pltpu.VMEM
    return pl.pallas_call(
        functools.partial(body, (n_sp, n_tp, R, fl, D, H, C, KV, NC)),
        out_shape=jax.ShapeDtypeStruct((TB, cd.shape[1]), BF),
        in_specs=[anys] * 11 + [vm] * 4,
        out_specs=vm,
        scratch_shapes=[
            V((R, D), BF), V((4, D, C), BF), V((D, H * LANES), BF), V((D, A), BF),
            V((D, KV + LANES), BF), V((C + A, cd.shape[1]), BF),
            V((n_sp, 2, RB, KV), BF), V((H, S, LANES), BF), V((H, S, LANES), BF),
            V((H, R, LANES), BF), V((R, LANES), F32), V((R, LANES), F32), V((R, LANES), F32),
            V((R, LANES), F32),
            V((R, C), BF), V((R, C), F32), V((R, A), F32), V((2, 16, C), BF), V((R, C + A), F32),
            V((H, RG, LANES), F32), V((H, RG, LANES), F32),
            V((X, TB, cd.shape[1]), BF), V((X, TB, cd.shape[1]), BF),
            V((X, TB, cd.shape[1]), BF), V((X, TB, cd.shape[1]), BF), V((TB, cd.shape[1]), BF),
            dma((11,)), dma((X, NC)), dma((X, NC)), dma((X, NC)), dma((X, NC)),
            dma((n_sp,)), dma((n_sp,)), dma((n_sp,)), dma((n_sp,)), dma((2,)), dma((2,)),
            dma((X,)), dma((X,)), dma((X,)), dma((X,)),
        ],
        compiler_params=pltpu.CompilerParams(
            collective_id=0, has_side_effects=True, vmem_limit_bytes=60 * 1024 * 1024),
    )(tokens, wci, wcn, wco, wcg, wq, wg, wl, wr, cd, ad, taps, gain.reshape(1, KV), ku, vu)


def solution(mesh):
    tp = P(None, "tp")
    placed = (P("sp", "tp"), tp, tp, tp, tp, tp, tp, P(), P(), P(), tp, tp, tp,
              P("tp", None), P("tp", None))
    return jax.shard_map(
        functools.partial(on_device, mesh.shape["sp"], mesh.shape["tp"]),
        mesh=mesh, in_specs=placed, out_specs=P(("sp", "tp"), None), check_vma=False)
```

time: 175 us -> 84.1 us (0.48)
  Pallas kernels: 0 us -> 71.8 us
  waiting for transfers between devices: 48.1 us -> 0 us
  matrix products: 45.5 us -> 0 us
  blocking collectives: 42.5 us -> 0 us
  between operations: 13.4 us -> 0.07 us
  loops' own time: 8.05 us -> 0 us
  local copies, waits for them, and re-layouts: 4.6 us -> 12 us
  other arithmetic: 7.14 us -> 0 us
  starting transfers between devices: 4.75 us -> 0 us
    pallas_call x0 -> x1, Pallas kernels: none -> 71.8 us  [on_device(): pl.pallas_call(functools.partial(body, (n_sp, n_tp, R, fl, D, H, C, KV, N...]
    dot_general x30 -> x0, matrix products: 45.5 us -> none  [the longest x8 9.98 us: on_device(): jnp.dot(shard_piece, matrix, preferred_element_type=jnp.float32)]
    all_gather x1 -> x0, blocking collectives: 34.1 us -> none  [on_device(): rope_piece = lax.all_gather(key_rope, 'sp', axis=0, tiled=True)]
    reduce_scatter x1 -> x0, waiting for transfers between devices: 30.1 us -> none  [on_device(): lax.psum_scatter((jnp.dot(conv_out, conv_down, preferred_element_type=jnp...]
    all_gather x2 -> x0, waiting for transfers between devices: 17.3 us -> none  [the longest x1 16.4 us: on_device(): shard_piece = lax.all_gather(tokens, 'tp', axis=1, tiled=True)]
    psum x1 -> x0, blocking collectives: 8.37 us -> none  [on_device(): squares = lax.psum(jnp.sum(widened * widened, axis=1), 'tp')]
    another operation x1 -> x0, loops' own time: 8.05 us -> none  [on_device(): gathered_state = lax.scan(one_span, initial, span_starts)[0]]
    reduce_sum x5 -> x0, other arithmetic: 5.68 us -> none  [the longest x4 4.46 us: one_span(): weight_total = weight_total * shrink + jnp.sum(weights, axis=2)]
  transfers between devices with their start and end apart: 5 -> 0, of which waited for: 3 -> 0; matrix products, arithmetic and copies ran while one was open for 7% -> 0% of each run, Pallas kernels for 0% -> 0%
where the time goes in v1:
time: 84.1 us; the launch traced here: 83.8 us
  Pallas kernels  71.8 us (85%)
  local copies, waits for them, and re-layouts  12 us (14%)
    pallas_call x1, Pallas kernels, on_device(): pl.pallas_call(functools.partial(body, (n_sp, n_tp, R, fl, D, H, C, KV, N...  71.8 us
    unnamed x11, local copies, waits for them, and re-layouts  5.02 us
    reshape x3, local copies, waits for them, and re-layouts, by_head(): jnp.pad(w, ((0, 0), (0, 0), (0, LANES - width)))  4.24 us

profile of v1, /device:TPU:0, one launch (start us, length us, event | category | flops | bytes accessed | tf_op | source)
XLA Modules:
  0.0 83.8 jit_solution(3794249009485093588)
XLA Ops:
  0.0 2.7 %copy.17 = bf16[2048,384]{0,1:T(8,128)(2,1)} copy(bf16[2048,384]{1,0:T(8,128)(2,1)} %param.21) | data formatting | bytes 3145728 | tf_op args[6]
  2.7 1.6 %pad.15 = bf16[2048,4,128]{0,2,1:T(8,128)(2,1)S(1)} pad(bf16[2048,4,96]{0,2,1:T(8,128)(2,1)} %bitcast.8, bf16[]{:T(256)} %constant.2.clone.1), padding=0_0x0_0x0_32 | pad | bytes 3670018 | tf_op jit(solution)/shard_map/jit(_pad)/pad | solution.py:393
  4.3 0.0 copy-start
  4.3 0.0 copy-start.1
  4.3 2.5 %copy.24.wq = bf16[2048,512]{1,0:T(8,128)(2,1)} copy(bf16[2048,512]{0,1:T(8,128)(2,1)S(1)} %bitcast.7) | data formatting | bytes 4194304 | tf_op jit(solution)/shard_map/reshape | solution.py:393
  6.8 0.0 copy-done
  6.9 0.0 copy-start.2
  6.9 0.3 copy.19
  7.1 1.0 %pad.16.wr = bf16[2048,128]{1,0:T(8,128)(2,1)} pad(bf16[2048,32]{1,0:T(8,128)(2,1)S(1)} %copy.19, bf16[]{:T(256)} %constant.2.clone.1), padding=0_0x64_32 | pad | bytes 655362 | tf_op jit(solution)/shard_map/jit(_pad)/pad | solution.py:398
  8.1 0.0 copy-done.1
  8.2 0.1 copy.20
  8.3 0.9 %copy.25.ku = bf16[256,512]{1,0:T(8,128)(2,1)} copy(bf16[256,512]{0,1:T(8,128)(2,1)S(1)} %bitcast.10) | data formatting | bytes 524288 | tf_op jit(solution)/shard_map/reshape | solution.py:393
  9.1 0.0 copy-done.2
  9.1 0.1 copy.22
  9.3 0.9 %copy.26.vu = bf16[256,512]{1,0:T(8,128)(2,1)} copy(bf16[256,512]{0,1:T(8,128)(2,1)S(1)} %bitcast.9) | data formatting | bytes 524288 | tf_op jit(solution)/shard_map/reshape | solution.py:393
  10.1 71.8 %shard_map.145 = bf16[128,2048]{1,0:T(8,128)(2,1)} custom-call(bf16[512,512]{1,0:T(8,128)(2,1)} %tokens.1, bf16[2048,256]{1,0:T(8,128)(2,1)} %wci.1, bf16[2048,256]{1,0:T(8,128)(2,1)} %wcn.1, bf16[2048,256]{1,0:T(8,128)(2,1)} %wco.1, bf16[2048,256]{1,0:T(8,128)(2,1)} %wcg.1, bf16[2048,512]{1,0:T(8,128)(2,1)} %copy.24.wq, bf16[2048,256]{1,0:T(8,128)(2,1)} %wg.1, ...), custom_call_target="tpu_custom_call" | custom-call | tf_op jit(solution)/shard_map/pallas_call | solution.py:406
  81.9 1.9 %copy.28 = bf16[128,2048]{1,0:T(8,128)(2,1)} copy(bf16[128,2048]{1,0:T(8,128)(2,1)} %shard_map.145) | data formatting | bytes 1048576
  (2 shorter events, 0.0 us)
Async XLA Ops:
  4.3 2.6 %copy-start = (bf16[2048,32]{0,1:T(8,128)(2,1)S(1)}, bf16[2048,32]{0,1:T(8,128)(2,1)}, u32[]{:S(2)}) copy-start(bf16[2048,32]{0,1:T(8,128)(2,1)} %param.23) | copy-start | bytes 393220
  4.3 3.8 %copy-start.1 = (bf16[256,256]{1,0:T(8,128)(2,1)S(1)}, bf16[256,256]{1,0:T(8,128)(2,1)}, u32[]{:S(2)}) copy-start(bf16[256,256]{1,0:T(8,128)(2,1)} %param.25) | copy-start | bytes 393220
  6.9 2.3 %copy-start.2 = (bf16[256,256]{1,0:T(8,128)(2,1)S(1)}, bf16[256,256]{1,0:T(8,128)(2,1)}, u32[]{:S(2)}) copy-start(bf16[256,256]{1,0:T(8,128)(2,1)} %param.26) | copy-start | bytes 393220

commit v2 on v1

--- a/solution.py
+++ b/solution.py
@@ -30,9 +30,9 @@
 
 def body(
     dims,
-    tokens, wci, wcn, wco, wcg, wq, wg, wl, wr, cd, ad, taps, gain, ku, vu,
+    tokens, wci, wcn, wco, wcg, wq, wg, wl, wr, cd, ad, ku, vu, taps, gain,
     out,
-    x_all, w_conv, w_q, w_g, w_lr, w_down, kv, kbuf, vbuf, qbuf, scl, cosb, sina, sinb,
+    x_all, w_conv, w_q, w_g, w_l, w_r, w_k, w_v, k_up, v_up, w_down, kv, kbuf, vbuf, qbuf, scl, cosb, sina, sinb,
     cprod, cgo, gat, halo, mix, mbuf, acc, sbuf, pbuf, xbuf, rbuf, ybuf,
     wsem, tsend, trecv, rsend, rrecv, ksend, krecv, psend, precv, hsend, hrecv,
     dsend, drecv, xsend, xrecv,
@@ -51,8 +51,8 @@
     mate = chip * 2 + (1 - core)
 
     loads = [
-        pltpu.make_async_copy(wl, w_lr.at[:, 0:KV], wsem.at[0]),
-        pltpu.make_async_copy(wr, w_lr.at[:, KV:KV + LANES], wsem.at[1]),
+        pltpu.make_async_copy(wl, w_l, wsem.at[0]),
+        pltpu.make_async_copy(wr, w_r, wsem.at[1]),
         pltpu.make_async_copy(wcn, w_conv.at[0], wsem.at[2]),
         pltpu.make_async_copy(wci, w_conv.at[1], wsem.at[3]),
         pltpu.make_async_copy(wco, w_conv.at[2], wsem.at[4]),
@@ -61,6 +61,8 @@
         pltpu.make_async_copy(wg, w_g, wsem.at[7]),
         pltpu.make_async_copy(cd, w_down.at[0:C, :], wsem.at[8]),
         pltpu.make_async_copy(ad, w_down.at[C:, :], wsem.at[9]),
+        pltpu.make_async_copy(ku, w_k, wsem.at[11]),
+        pltpu.make_async_copy(vu, w_v, wsem.at[12]),
     ]
 
     def cols(j):
@@ -135,12 +137,13 @@
         xf = xr.astype(F32)
         sc = lax.rsqrt(jnp.sum(xf * xf, axis=1, keepdims=True) * (1.0 / D) + rms_eps)
         scl[rows, :] = jnp.broadcast_to(sc, (RC, LANES))
-        z = dot(xr, w_lr[...]) * sc
-        lat = z[:, :KV]
+        lat = dot(xr, w_l[...]) * sc
         lat = lat * lax.rsqrt(jnp.mean(lat * lat, axis=1, keepdims=True) + rms_eps) * gain[...]
         half, off = (c * RC) // HB, (c * RC) % HB
         kv[sp, half, off:off + RC, :] = lat.astype(BF)
-        rp = z[:, KV:]
+        rp = jnp.concatenate([jnp.zeros((RC, NOPE), F32), lax.dot_general(
+            xr, w_r[...], (((1,), (1,)), ((), ())), preferred_element_type=F32) * sc,
+                              jnp.zeros((RC, LANES - NOPE - ROPE), F32)], axis=1)
         mix[rows, 0:LANES] = rp * cosb[rows, :] + turned(rp, rows)
     for half in range(2):
         packed = []
@@ -193,6 +196,7 @@
         cgo[rows, :] = silu(gate) * outer
 
     EDGE = 16
+    HW = NOPE + ROPE
 
     def send_halo(k):
         src = cprod.at[pl.ds(R - EDGE, EDGE)] if k == 0 else cprod.at[pl.ds(0, EDGE)]
@@ -203,6 +207,14 @@
 
     send_halo(0).start()
     send_halo(1).start()
+    def origin(s):
+        step = jnp.where(s % 2 == 1, (s + 1) // 2, n_sp - s // 2)
+        return (sp + step) % n_sp
+
+    o1 = origin(1)
+    recv_kv(o1).wait_recv()
+    relay_kv(o1, core).start()
+
     loads[6].wait()
     loads[7].wait()
 
@@ -214,10 +226,18 @@
         q = dot(xr, w_q[...]) * sc
         ln = lax.broadcasted_iota(jnp.int32, (PB, LANES), 1)
         for h in range(H):
-            v = q[:, h * LANES:(h + 1) * LANES]
+            v = jnp.concatenate([q[:, h * HW:(h + 1) * HW], jnp.zeros((PB, LANES - HW), F32)], axis=1)
             v = v * jnp.where(ln < NOPE, 1.0, cosb[rows, :]) + turned(v, rows)
             qbuf[h, rows, :] = v.astype(BF)
         gat[rows, :] = silu((dot(xr, w_g[...]) * sc).astype(BF).astype(F32))
+
+    loads[10].wait()
+    loads[11].wait()
+    for h in range(H):
+        for raw, wide, width in ((w_k, k_up, NOPE), (w_v, v_up, VDIM)):
+            piece = raw[:, h * width:(h + 1) * width].astype(F32)
+            pad = jnp.zeros((KV, LANES - width), F32)
+            wide[:, h * LANES:(h + 1) * LANES] = jnp.concatenate([piece, pad], axis=1).astype(BF)
 
     def build(o):
         ln = lax.broadcasted_iota(jnp.int32, (HR, LANES), 1)
@@ -232,14 +252,14 @@
                 for b in range(4):
                     parts.append(jnp.where(keep, pltpu.roll(pg, (NOPE - 32 * b) % LANES, 1), 0.0))
             rope = jnp.concatenate(parts, axis=0)
-            k = dot(lat, ku[...])
-            v = dot(lat, vu[...])
+            k = dot(lat, k_up[...])
+            v = dot(lat, v_up[...])
             rows = pl.ds(pl.multiple_of(o * R + half * HB, HB), HB)
             for h in range(H):
                 kbuf[h, rows, :] = (k[:, h * LANES:(h + 1) * LANES] + rope).astype(BF)
                 vbuf[h, rows, :] = (v[:, h * LANES:(h + 1) * LANES] + ones).astype(BF)
 
-    scale = (NOPE + ROPE) ** -0.5
+    scale = (NOPE + ROPE) ** -0.5 * math.log2(math.e)
 
     def attend(row0, key0, count):
         qrows = pl.ds(row0, RG)
@@ -249,8 +269,8 @@
                                 preferred_element_type=F32)
             old = mbuf[h]
             new = jnp.maximum(old, jnp.max(s, axis=1, keepdims=True))
-            p = jnp.exp((s - new[:, 0:1]) * scale)
-            shrink = jnp.exp((old - new) * scale)
+            p = jnp.exp2((s - new[:, 0:1]) * scale)
+            shrink = jnp.exp2((old - new) * scale)
             acc[h] = acc[h] * shrink + dot(p.astype(BF), vbuf[h, krows, :])
             mbuf[h] = new
 
@@ -270,10 +290,6 @@
     def row_of(k):
         return pl.multiple_of(k * RG, RG)
 
-    def origin(s):
-        step = jnp.where(s % 2 == 1, (s + 1) // 2, n_sp - s // 2)
-        return (sp + step) % n_sp
-
     def block(k, which):
         rows = pl.ds(pl.multiple_of(k * RG + which * TB, TB), TB)
         return dot(mix[rows, :].astype(BF), w_down[...])
@@ -302,10 +318,6 @@
     reset()
     build(sp)
     attend(first_chip, pl.multiple_of(sp * R, R), R)
-
-    o1 = origin(1)
-    recv_kv(o1).wait_recv()
-    relay_kv(o1, core).start()
 
     @pl.loop(1, n_sp)
     def _(s):
@@ -388,14 +400,6 @@
     RG, TB = R // X, R // n_tp
     NC = 4
 
-    def by_head(w, width):
-        w = w.reshape(w.shape[0], H, width)
-        return jnp.pad(w, ((0, 0), (0, 0), (0, LANES - width))).reshape(w.shape[0], H * LANES)
-
-    wq = by_head(wq, NOPE + ROPE)
-    ku = by_head(ku, NOPE)
-    vu = by_head(vu, VDIM)
-    wr = jnp.pad(wr, ((0, 0), (NOPE, LANES - NOPE - ROPE)))
     HB = R // 2
     RB = HB + HB // 8
     S = n_sp * R
@@ -406,11 +410,12 @@
     return pl.pallas_call(
         functools.partial(body, (n_sp, n_tp, R, fl, D, H, C, KV, NC)),
         out_shape=jax.ShapeDtypeStruct((TB, cd.shape[1]), BF),
-        in_specs=[anys] * 11 + [vm] * 4,
+        in_specs=[anys] * 13 + [vm] * 2,
         out_specs=vm,
         scratch_shapes=[
-            V((R, D), BF), V((4, D, C), BF), V((D, H * LANES), BF), V((D, A), BF),
-            V((D, KV + LANES), BF), V((C + A, cd.shape[1]), BF),
+            V((R, D), BF), V((4, D, C), BF), V(wq.shape, BF), V((D, A), BF),
+            V((D, KV), BF), V((ROPE, D), BF), V(ku.shape, BF), V(vu.shape, BF),
+            V((KV, H * LANES), BF), V((KV, H * LANES), BF), V((C + A, cd.shape[1]), BF),
             V((n_sp, 2, RB, KV), BF), V((H, S, LANES), BF), V((H, S, LANES), BF),
             V((H, R, LANES), BF), V((R, LANES), F32), V((R, LANES), F32), V((R, LANES), F32),
             V((R, LANES), F32),
@@ -418,13 +423,13 @@
             V((H, RG, LANES), F32), V((H, RG, LANES), F32),
             V((X, TB, cd.shape[1]), BF), V((X, TB, cd.shape[1]), BF),
             V((X, TB, cd.shape[1]), BF), V((X, TB, cd.shape[1]), BF), V((TB, cd.shape[1]), BF),
-            dma((11,)), dma((X, NC)), dma((X, NC)), dma((X, NC)), dma((X, NC)),
+            dma((13,)), dma((X, NC)), dma((X, NC)), dma((X, NC)), dma((X, NC)),
             dma((n_sp,)), dma((n_sp,)), dma((n_sp,)), dma((n_sp,)), dma((2,)), dma((2,)),
             dma((X,)), dma((X,)), dma((X,)), dma((X,)),
         ],
         compiler_params=pltpu.CompilerParams(
             collective_id=0, has_side_effects=True, vmem_limit_bytes=60 * 1024 * 1024),
-    )(tokens, wci, wcn, wco, wcg, wq, wg, wl, wr, cd, ad, taps, gain.reshape(1, KV), ku, vu)
+    )(tokens, wci, wcn, wco, wcg, wq, wg, wl, wr.T, cd, ad, ku, vu, taps, gain.reshape(1, KV))
 
 
 def solution(mesh):

time: 84.1 us -> 73.4 us (0.87)
  local copies, waits for them, and re-layouts: 12 us -> 1.88 us
    reshape x3 -> x0, local copies, waits for them, and re-layouts: 4.24 us -> none  [by_head(): jnp.pad(w, ((0, 0), (0, 0), (0, LANES - width)))]
    unnamed x11 -> x1, local copies, waits for them, and re-layouts: 5.02 us -> 1.88 us
    pad x4 -> x0, local copies, waits for them, and re-layouts: 2.69 us -> none  [the longest x3 1.67 us: by_head(): jnp.pad(w, ((0, 0), (0, 0), (0, LANES - width)))]
where the time goes in v2:
time: 73.4 us; the launch traced here: 73.2 us
  Pallas kernels  71.3 us (97%)
  local copies, waits for them, and re-layouts  1.88 us (3%)
    pallas_call x1, Pallas kernels, on_device(): pl.pallas_call(functools.partial(body, (n_sp, n_tp, R, fl, D, H, C, KV, N...  71.3 us
    unnamed x1, local copies, waits for them, and re-layouts  1.88 us

profile of v2, /device:TPU:0, one launch (start us, length us, event | category | flops | bytes accessed | tf_op | source)
XLA Modules:
  0.0 73.2 jit_solution(16383067272236447399)
XLA Ops:
  0.0 71.3 %shard_map.145 = bf16[128,2048]{1,0:T(8,128)(2,1)} custom-call(bf16[512,512]{1,0:T(8,128)(2,1)} %tokens.1, bf16[2048,256]{1,0:T(8,128)(2,1)} %wci.1, bf16[2048,256]{1,0:T(8,128)(2,1)} %wcn.1, bf16[2048,256]{1,0:T(8,128)(2,1)} %wco.1, bf16[2048,256]{1,0:T(8,128)(2,1)} %wcg.1, bf16[2048,384]{1,0:T(8,128)(2,1)} %wq.1, bf16[2048,256]{1,0:T(8,128)(2,1)} %wg.1, ...), custom_call_target="tpu_custom_call" | custom-call | tf_op jit(solution)/shard_map/pallas_call | solution.py:410
  71.3 1.9 %copy.17 = bf16[128,2048]{1,0:T(8,128)(2,1)} copy(bf16[128,2048]{1,0:T(8,128)(2,1)} %shard_map.145) | data formatting | bytes 1048576
